TPU v7x, 256 devices: a whole 4x4x8 slice. The times are simulated.
256 devices in a mesh: kv: 16 (over y, x), tp: 16 (over z, core).
Axes of the slice: x: 4, y: 4, z: 8, core: 2. Of those that a mesh axis runs over, the one named last changes fastest.
Arguments:
- tokens: bfloat16 [256, 4096], P('kv', 'tp'), may hold values from -6 to 6
- attn_gain: float32 [4096], replicated, may hold values from 0.1 to 1.9
- w_query: bfloat16 [4096, 2048], P(None, 'tp'), may hold values from -0.09375 to 0.09375
- w_key: bfloat16 [4096, 2048], P(None, 'tp'), may hold values from -0.09375 to 0.09375
- w_value: bfloat16 [4096, 2048], P(None, 'tp'), may hold values from -0.09375 to 0.09375
- w_outgate: bfloat16 [4096, 2048], P(None, 'tp'), may hold values from -0.09375 to 0.09375
- w_rates: bfloat16 [2, 4096, 16], P(None, None, 'tp'), may hold values from -0.09375 to 0.09375
- head_rate: float32 [16], P('tp'), may hold values from 0.02 to 2
- head_gain: float32 [2048], P('tp'), may hold values from 0.1 to 1.9
- w_out: bfloat16 [2048, 4096], P('tp'), may hold values from -0.125 to 0.125
- state: float32 [256, 16, 128, 128], P('kv', 'tp'), may hold values from -2.4 to 2.4
- mlp_gain: float32 [4096], replicated, may hold values from 0.1 to 1.9
- w_gate: bfloat16 [4096, 11264], P(None, ('kv', 'tp')), may hold values from -0.09375 to 0.09375
- w_up: bfloat16 [4096, 11264], P(None, ('kv', 'tp')), may hold values from -0.09375 to 0.09375
- w_down: bfloat16 [4096, 11264], P(None, ('kv', 'tp')), may hold values from -0.25 to 0.25
Outputs:
- result: bfloat16 [256, 4096], P('kv', 'tp')
- new_state: float32 [256, 16, 128, 128], P('kv', 'tp')
All inputs are finite; a program needn't handle non-finite values.
Results may differ from a plain program's by a relative error of at most 0.014.
Values may be sent and summed in bfloat16 or wider, within the bound.
A program may use at most 64 MiB of HBM per device.

v0:
```python
import jax
import jax.numpy as jnp
from jax import lax
from jax.sharding import PartitionSpec as P

EPS = 1e-06


def copy_for_each(value, axis):
    size = lax.axis_size(axis)
    return lax.all_to_all(
        jnp.broadcast_to(value[None], (size, *value.shape)), axis, 0, 0, tiled=True
    )


def in_order(tiles, dim):
    lengths = list(tiles.shape[1:])
    lengths[dim] *= tiles.shape[0]
    return jnp.moveaxis(tiles, 0, dim).reshape(lengths)


def gather_directly(value, axis, dim):
    tiles = copy_for_each(value, axis)
    return in_order(tiles, dim)


def cut_along(value, dim, size):
    lengths = value.shape
    tiles = value.reshape(*lengths[:dim], size, lengths[dim] // size, *lengths[dim + 1 :])
    return jnp.moveaxis(tiles, dim, 0)


def sent_and_summed(value, axis, dim):
    size = lax.axis_size(axis)
    tiles = lax.all_to_all(cut_along(value, dim, size), axis, 0, 0, tiled=True)
    return jnp.sum(tiles.astype(jnp.float32), axis=0)


def sent_and_summed_2(value, axis, dim):
    tiles = cut_along(value, dim, lax.axis_size(axis))
    arrived = lax.all_to_all(tiles, axis, split_axis=0, concat_axis=0, tiled=True)
    return arrived.sum(axis=0)


def row_norm(values, gain):
    floats = values.astype(jnp.float32)
    scaled = floats * lax.rsqrt(jnp.mean(floats * floats, axis=-1, keepdims=True) + EPS)
    return (scaled * gain).astype(jnp.bfloat16)


def hidden_units(normed_mlp, gate_part, up_part):
    gate_pre = jnp.dot(normed_mlp, gate_part, preferred_element_type=jnp.float32)
    up_pre = jnp.dot(normed_mlp, up_part, preferred_element_type=jnp.float32)
    return (jax.nn.silu(gate_pre) * up_pre).astype(jnp.bfloat16)


def down_product(hidden, down_part):
    return lax.dot_general(
        hidden, down_part, (((1,), (1,)), ((), ())), preferred_element_type=jnp.float32
    )


def body(
    tokens,
    attn_gain,
    w_query,
    w_key,
    w_value,
    w_outgate,
    w_rates,
    head_rate,
    head_gain,
    w_out,
    state,
    mlp_gain,
    w_gate,
    w_up,
    w_down,
):
    count = tokens.shape[0]
    local_heads = head_rate.shape[0]
    size = w_query.shape[1] // local_heads
    whole_rows = gather_directly(tokens, "tp", 1)
    normed = row_norm(whole_rows, attn_gain)
    query = jnp.dot(normed, w_query, preferred_element_type=jnp.float32).reshape(
        count, local_heads, size
    )
    key = jnp.dot(normed, w_key, preferred_element_type=jnp.float32).reshape(
        count, local_heads, size
    )
    value = jnp.dot(normed, w_value, preferred_element_type=jnp.float32).reshape(
        count, local_heads, size
    )
    gate_in = jnp.dot(normed, w_outgate, preferred_element_type=jnp.float32).reshape(
        count, local_heads, size
    )
    rates = jnp.einsum("bd,sdh->sbh", normed, w_rates, preferred_element_type=jnp.float32)
    unit_query = (
        query * lax.rsqrt(jnp.sum(query * query, axis=-1, keepdims=True) + EPS) * size ** (-0.5)
    )
    unit_key = key * lax.rsqrt(jnp.sum(key * key, axis=-1, keepdims=True) + EPS)
    strength = jax.nn.sigmoid(rates[0])
    fade = jnp.exp(-head_rate * jax.nn.softplus(rates[1]))
    carried = state * fade[:, :, None, None]
    fresh = strength[:, :, None] * (value - jnp.einsum("bhi,bhiv->bhv", unit_key, carried))
    new_state = carried + unit_key[:, :, :, None] * fresh[:, :, None, :]
    readout = jnp.einsum("bhi,bhiv->bhv", unit_query, new_state)
    normed_out = readout * lax.rsqrt(jnp.mean(readout * readout, axis=-1, keepdims=True) + EPS)
    mixed = (normed_out * head_gain.reshape(local_heads, size) * jax.nn.silu(gate_in)).astype(
        jnp.bfloat16
    )
    partial_value = jnp.dot(
        mixed.reshape(count, local_heads * size), w_out, preferred_element_type=jnp.float32
    )
    projected = sent_and_summed(partial_value.astype(jnp.bfloat16), "tp", 1)
    residual = (tokens.astype(jnp.float32) + projected).astype(jnp.bfloat16)
    full_residual = gather_directly(residual, "tp", 1)
    normed_mlp = row_norm(full_residual, mlp_gain)
    shared_rows = gather_directly(normed_mlp, "kv", 0)
    hidden = hidden_units(shared_rows, w_gate, w_up)
    owned = lax.all_to_all(hidden, "kv", split_axis=0, concat_axis=1, tiled=True)
    folded = down_product(owned, lax.all_gather(w_down, "kv", axis=1, tiled=True))
    down = sent_and_summed_2(folded, "tp", 1)
    result = (residual.astype(jnp.float32) + down).astype(jnp.bfloat16)
    return (result, new_state)


def solution(mesh):
    return jax.shard_map(
        body,
        mesh=mesh,
        in_specs=(
            P("kv", "tp"),
            P(),
            P(None, "tp"),
            P(None, "tp"),
            P(None, "tp"),
            P(None, "tp"),
            P(None, None, "tp"),
            P("tp"),
            P("tp"),
            P("tp", None),
            P("kv", "tp", None, None),
            P(),
            P(None, ("kv", "tp")),
            P(None, ("kv", "tp")),
            P(None, ("kv", "tp")),
        ),
        out_specs=(P("kv", "tp"), P("kv", "tp", None, None)),
        check_vma=False,
    )
```

profile of v0, /device:TPU:1, one launch (start us, length us, event | category | flops | bytes accessed | tf_op | source)
XLA Modules:
  0.0 156.5 jit_solution(1678312154421125208)
XLA Ops:
  7.2 0.0 copy-start
  7.2 0.0 copy-start.8
  7.2 0.0 copy-start.2
  7.2 0.0 all-gather.3.cloned.1.call-start
  7.2 0.7 all-gather.3.cloned.1.call-update
  7.9 1.4 broadcast_in_dim.6
  9.3 10.0 %all-to-all-start = ((bf16[16,16,256]{2,1,0:T(8,128)(2,1)}), bf16[16,16,256]{2,1,0:T(8,128)(2,1)S(1)}, u32[]{:S(2)}, u32[]{:S(2)}) async-start(bf16[16,16,256]{2,1,0:T(8,128)(2,1)} %broadcast_in_dim.6), calls=%async_computation | async-start | bytes 262144 | tf_op jit(solution)/shard_map/all_to_all | solution.py:11
  19.9 0.7 mul.205
  20.6 7.5 %all-to-all-done = bf16[16,16,256]{2,1,0:T(8,128)(2,1)S(1)} async-done(((bf16[16,16,256]{2,1,0:T(8,128)(2,1)}), bf16[16,16,256]{2,1,0:T(8,128)(2,1)S(1)}, u32[]{:S(2)}, u32[]{:S(2)}) %all-to-all-start) | async-done | bytes 131104 | tf_op jit(solution)/shard_map/all_to_all | solution.py:11
  28.2 0.0 copy-start.3
  28.2 0.1 fusion.15
  28.3 0.0 copy-start.12
  28.3 0.1 fusion.18
  28.4 0.0 copy-start.1
  28.5 0.0 copy-start.4
  28.5 0.0 copy-done.8
  28.5 0.1 multiply_convert_fusion.1
  28.6 0.0 copy-done.2
  28.6 0.4 multiply_reduce_fusion.1
  29.0 0.4 copy-done.3
  29.4 0.0 copy-start.5
  29.4 0.0 copy-start.11
  29.4 0.4 multiply_reduce_fusion.2
  29.8 0.0 copy-done.12
  29.8 0.2 convolution_bitcast_fusion
  30.0 0.1 broadcast_multiply_fusion
  30.1 0.1 multiply_multiply_fusion
  30.1 0.0 copy-done.1
  30.1 0.3 fusion.10
  30.4 0.0 copy-done.4
  30.4 0.3 fusion.7
  30.7 0.0 copy-start.9
  30.7 0.5 fusion.33
  31.2 0.1 multiply_reduce_fusion
  31.3 0.0 copy-done
  31.3 0.0 copy-done.5
  31.3 0.0 copy-done.11
  31.4 0.0 copy-start.10
  31.4 0.5 convolution_convert_fusion
  31.9 11.6 %all_to_all.44 = bf16[16,16,256]{2,1,0:T(8,128)(2,1)S(1)} all-to-all(bf16[16,16,256]{2,1,0:T(8,128)(2,1)S(1)} %bitcast.108), channel_id=1, replica_groups=mesh['kv'=16,'tp'=16] {'tp'}, dimensions={0} | all-to-all | bytes 262144 | tf_op jit(solution)/shard_map/all_to_all | solution.py:35
  43.5 0.0 copy-done.9
  43.5 11.6 %all_to_all.45 = bf16[16,16,256]{2,1,0:T(8,128)(2,1)S(1)} all-to-all(bf16[16,16,256]{2,1,0:T(8,128)(2,1)S(1)} %broadcast_in_dim.7), channel_id=1, replica_groups=mesh['kv'=16,'tp'=16] {'tp'}, dimensions={0} | all-to-all | bytes 262144 | tf_op jit(solution)/shard_map/all_to_all | solution.py:11
  55.1 0.1 fusion.14
  55.3 0.0 copy-done.10
  55.3 0.1 multiply_convert_fusion
  55.4 0.2 broadcast_in_dim.8
  55.6 0.0 copy-start.6
  55.6 49.6 %all_to_all.46 = bf16[16,16,4096]{2,1,0:T(8,128)(2,1)S(1)} all-to-all(bf16[16,16,4096]{2,1,0:T(8,128)(2,1)S(1)} %broadcast_in_dim.8), channel_id=1, replica_groups=mesh['kv'=16,'tp'=16] {'kv'}, dimensions={0} | all-to-all | bytes 4194304 | tf_op jit(solution)/shard_map/all_to_all | solution.py:11
  105.2 0.0 copy-done.6
  105.2 0.7 fusion.36
  106.0 0.2 copy-done.7
  106.2 0.7 fusion.6
  107.0 0.1 copy.25
  107.1 0.1 reshape.265
  107.3 9.0 %all_to_all.47 = bf16[16,2,352]{2,1,0:T(2,128)(2,1)S(1)} all-to-all(bf16[16,2,352]{2,1,0:T(2,128)(2,1)S(1)} %reshape.265), channel_id=1, replica_groups=mesh['kv'=16,'tp'=16] {'kv'}, dimensions={0} | all-to-all | bytes 45056 | tf_op jit(solution)/shard_map/all_to_all | solution.py:121
  116.3 0.1 reshape.266
  116.4 0.1 reshape.263
  116.5 0.0 all-gather.3.cloned.1.call-done
  116.5 8.0 %reshape.258 = bf16[704,4096]{1,0:T(8,128)(2,1)} reshape(bf16[16,44,4096]{2,1,0:T(8,128)(2,1)} %all-gather.3.cloned.1.call-done) | data formatting | bytes 11534336
  124.6 4.2 %fusion.3 = f32[16,16,256]{2,1,0:T(8,128)} fusion(bf16[16,704,1]{1,0,2:T(8,128)(2,1)S(1)} %reshape.263, bf16[88,16,8,256]{3,2,1,0:T(8,128)(2,1)} %bitcast.102), kind=kOutput, calls=%fused_computation.4 | convolution fusion | flops 92274688 | bytes 6051840 | tf_op jit(solution)/shard_map/dot_general | solution.py:58
  128.8 8.7 %all-to-all-start.5 = ((f32[16,16,256]{2,1,0:T(8,128)}), f32[16,16,256]{2,1,0:T(8,128)S(1)}, u32[]{:S(2)}, u32[]{:S(2)}) async-start(f32[16,16,256]{2,1,0:T(8,128)} %fusion.3), calls=%async_computation.5 | async-start | bytes 524288 | tf_op jit(solution)/shard_map/all_to_all | solution.py:41
  137.5 1.3 multiply_add_fusion
  138.8 10.3 %all-to-all-done.5 = f32[16,16,256]{2,1,0:T(8,128)S(1)} async-done(((f32[16,16,256]{2,1,0:T(8,128)}), f32[16,16,256]{2,1,0:T(8,128)S(1)}, u32[]{:S(2)}, u32[]{:S(2)}) %all-to-all-start.5) | async-done | bytes 262176 | tf_op jit(solution)/shard_map/all_to_all | solution.py:41
  149.1 0.6 add_convert_fusion
  (19 shorter events, 0.3 us)
Async XLA Ops:
  7.2 24.2 %copy-start = (bf16[128,4096]{1,0:T(8,128)(2,1)S(1)}, bf16[128,4096]{1,0:T(8,128)(2,1)}, u32[]{:S(2)}) copy-start(bf16[128,4096]{1,0:T(8,128)(2,1)} %param.24) | copy-start | bytes 3145732
  7.2 21.3 %copy-start.8 = (f32[4096]{0:T(1024)S(1)}, f32[4096]{0:T(1024)}, u32[]{:S(2)}) copy-start(f32[4096]{0:T(1024)} %param.16) | copy-start | bytes 49156
  7.2 21.4 %copy-start.2 = (bf16[4096,128]{1,0:T(8,128)(2,1)S(1)}, bf16[4096,128]{1,0:T(8,128)(2,1)}, u32[]{:S(2)}) copy-start(bf16[4096,128]{1,0:T(8,128)(2,1)} %param.18) | copy-start | bytes 3145732
  7.2 109.3 %all-gather.3.cloned.1.call-start = ((), (), s32[]{:S(2)}) async-start(), calls=%async_computation.6 | async-start | bytes 6684672 | tf_op jit(solution)/shard_map/all_gather | solution.py:122
  9.3 18.9 %all-to-all-start = ((bf16[16,16,256]{2,1,0:T(8,128)(2,1)}), bf16[16,16,256]{2,1,0:T(8,128)(2,1)S(1)}, u32[]{:S(2)}, u32[]{:S(2)}) async-start(bf16[16,16,256]{2,1,0:T(8,128)(2,1)} %broadcast_in_dim.6), calls=%async_computation | async-start | bytes 262144 | tf_op jit(solution)/shard_map/all_to_all | solution.py:11
  28.2 1.2 copy-start.3
  28.3 1.4 copy-start.12
  28.4 1.7 %copy-start.1 = (f32[16,1,128,128]{3,2,1,0:T(8,128)S(1)}, f32[16,1,128,128]{3,2,1,0:T(8,128)}, u32[]{:S(2)}) copy-start(f32[16,1,128,128]{3,2,1,0:T(8,128)} %param.25) | copy-start | bytes 3145732
  28.5 1.9 %copy-start.4 = (bf16[4096,128]{1,0:T(8,128)(2,1)S(1)}, bf16[4096,128]{1,0:T(8,128)(2,1)}, u32[]{:S(2)}) copy-start(bf16[4096,128]{1,0:T(8,128)(2,1)} %param.19) | copy-start | bytes 3145732
  29.4 2.0 %copy-start.5 = (bf16[4096,128]{1,0:T(8,128)(2,1)S(1)}, bf16[4096,128]{1,0:T(8,128)(2,1)}, u32[]{:S(2)}) copy-start(bf16[4096,128]{1,0:T(8,128)(2,1)} %param.20) | copy-start | bytes 3145732
  29.4 2.0 %copy-start.11 = (f32[128]{0:T(128)S(1)}, f32[128]{0:T(128)}, u32[]{:S(2)}) copy-start(f32[128]{0:T(128)} %param.23) | copy-start | bytes 1540
  30.7 12.8 %copy-start.9 = (bf16[16,256]{1,0:T(8,128)(2,1)S(1)}, bf16[16,256]{1,0:T(8,128)(2,1)}, u32[]{:S(2)}) copy-start(bf16[16,256]{1,0:T(8,128)(2,1)} %param.15) | copy-start | bytes 24580
  31.4 23.9 %copy-start.10 = (f32[4096]{0:T(1024)S(1)}, f32[4096]{0:T(1024)}, u32[]{:S(2)}) copy-start(f32[4096]{0:T(1024)} %param.26) | copy-start | bytes 49156
  55.6 49.6 %copy-start.6 = (bf16[4096,44]{0,1:T(8,128)(2,1)S(1)}, bf16[4096,44]{0,1:T(8,128)(2,1)}, u32[]{:S(2)}) copy-start(bf16[4096,44]{0,1:T(8,128)(2,1)} %param.27) | copy-start | bytes 1081348
  105.2 1.0 copy-start.7
  128.8 20.3 %all-to-all-start.5 = ((f32[16,16,256]{2,1,0:T(8,128)}), f32[16,16,256]{2,1,0:T(8,128)S(1)}, u32[]{:S(2)}, u32[]{:S(2)}) async-start(f32[16,16,256]{2,1,0:T(8,128)} %fusion.3), calls=%async_computation.5 | async-start | bytes 524288 | tf_op jit(solution)/shard_map/all_to_all | solution.py:41
Sparse Core Ops, SparseCore 0:
  10.4 91.6 all-gather.2
where the time goes:
time: 157 us
  blocking collectives  81.7 us (52%)
  starting transfers between devices  18.7 us (12%)
  waiting for transfers between devices  18.5 us (12%)
  between operations  15 us (10%)
  local copies, waits for them, and re-layouts  11.6 us (7%)
  matrix products  8.08 us (5%)
  other arithmetic  2.96 us (2%)
    all_to_all x2, blocking collectives, copy_for_each(): lax.all_to_all(jnp.broadcast_to(value[None], (size, *value.shape)), axis,...  61.2 us
    all_to_all x1, blocking collectives, sent_and_summed(): tiles = lax.all_to_all(cut_along(value, dim, size), axis, 0, 0, tiled=True)  11.6 us
    all_to_all x1, waiting for transfers between devices, sent_and_summed_2(): lax.all_to_all(tiles, axis, split_axis=0, concat_axis=0, tiled=True)  10.3 us
    all_to_all x1, starting transfers between devices, copy_for_each(): lax.all_to_all(jnp.broadcast_to(value[None], (size, *value.shape)), axis,...  9.97 us
    all_to_all x1, blocking collectives, body(): lax.all_to_all(hidden, 'kv', split_axis=0, concat_axis=1, tiled=True)  8.99 us
    unnamed x29, local copies, waits for them, and re-layouts  8.94 us
    all_to_all x1, starting transfers between devices, sent_and_summed_2(): lax.all_to_all(tiles, axis, split_axis=0, concat_axis=0, tiled=True)  8.69 us
    all_to_all x1, waiting for transfers between devices, copy_for_each(): lax.all_to_all(jnp.broadcast_to(value[None], (size, *value.shape)), axis,...  7.51 us
  transfers between devices with their start and end apart: 3, of which 2 were waited for; matrix products, arithmetic and copies ran while one was open for 6% of the time, Pallas kernels for 0%

commit v1 on v0

v1 whole, which is shorter than its diff:
```python
import math

import jax
import jax.numpy as jnp
from jax import lax
from jax.experimental import pallas as pl
from jax.experimental.pallas import tpu as pltpu
from jax.sharding import PartitionSpec as P

EPS = 1e-06
MESH = pl.DeviceIdType.MESH
F32 = jnp.float32
BF16 = jnp.bfloat16


def layer_kernel(
    n_side,
    n_z,
    tok_hbm,
    again_ref,
    wq_hbm,
    wk_hbm,
    wv_hbm,
    wo_hbm,
    wrates_ref,
    hrate_ref,
    hgain_ref,
    wout_hbm,
    state_hbm,
    mgain_ref,
    wgate_hbm,
    wup_hbm,
    wdown_hbm,
    result_ref,
    ns_hbm,
    tok_own,
    tok_all,
    wqkvg,
    wout,
    state,
    ns,
    pred,
    own_w,
    far_w,
    gu,
    wd,
    part1,
    recv1,
    ag,
    ex_out,
    ex_in,
    pb,
    ra1,
    ra2,
    rb1,
    rb2,
    mid_a,
    mid_b,
    zout,
    zin,
    local_sem,
    loc_w_sem,
    far_send_sem,
    far_recv_sem,
    tok_send_sem,
    tok_recv_sem,
    p1_send_sem,
    p1_recv_sem,
    agz_send_sem,
    agz_recv_sem,
    ag_send_sem,
    ag_recv_sem,
    ex_send_sem,
    ex_recv_sem,
    r1_send_sem,
    r1_recv_sem,
    r2_send_sem,
    r2_recv_sem,
    rz_send_sem,
    rz_recv_sem,
):
    n_tp = 2 * n_z
    half = n_z // 2
    rows, fpd = tok_own.shape
    head = hgain_ref.shape[1]
    units = wgate_hbm.shape[0]
    upad = gu.shape[0] // 4
    me_k = lax.axis_index("kv")
    me_t = lax.axis_index("tp")
    my_y, my_x = me_k // n_side, lax.rem(me_k, n_side)
    my_z, my_c = me_t // 2, lax.rem(me_t, 2)
    partner = me_t + 1 - 2 * my_c

    def z_at(d):
        return lax.rem(my_z + d, n_z)

    def y_at(d):
        return lax.rem(my_y + d, n_side)

    def x_at(d):
        return lax.rem(my_x + d, n_side)

    def tp_id(t):
        return {"tp": t}

    def kv_id(y, x):
        return {"kv": y * n_side + x}

    def remote(src, dst, send, recv, device):
        return pltpu.make_async_remote_copy(
            src_ref=src,
            dst_ref=dst,
            send_sem=send,
            recv_sem=recv,
            device_id=device,
            device_id_type=MESH,
        )

    near = [0]
    for d in range(1, n_z // 2):
        near += [d, n_z - d]
    near += [n_z // 2]
    others = [(d, c) for d in near for c in (0, 1)][1:]

    def tp_at(d, flip):
        c = (1 - my_c) if flip else my_c
        return z_at(d) * 2 + c

    tok_copy = pltpu.make_async_copy(tok_hbm, tok_own, local_sem.at[0])
    tok_copy.start()
    w_copies = []
    for j, src in enumerate((wq_hbm, wk_hbm, wv_hbm, wo_hbm)):
        cp = pltpu.make_async_copy(
            src, wqkvg.at[:, pl.ds(j * head, head)], local_sem.at[1 + j]
        )
        cp.start()
        w_copies.append(cp)
    state_copy = pltpu.make_async_copy(state_hbm, state, local_sem.at[5])
    state_copy.start()
    wout_copy = pltpu.make_async_copy(wout_hbm, wout, local_sem.at[6])
    wout_copy.start()
    own_copies = []
    mats = (wgate_hbm, wup_hbm, wdown_hbm)
    for j, src in enumerate(mats):
        for zz in range(n_z):
            cols = pl.ds(pl.multiple_of((2 * zz + my_c) * fpd, fpd), fpd)
            cp = pltpu.make_async_copy(src.at[:, cols], own_w.at[j, zz], loc_w_sem.at[j, zz])
            cp.start()
            own_copies.append(cp)

    barrier = pltpu.get_barrier_semaphore()
    for d, flip in others:
        pl.semaphore_signal(
            barrier, inc=1, device_id=tp_id(tp_at(d, flip)), device_id_type=MESH
        )
    for d in range(1, n_side):
        pl.semaphore_signal(
            barrier, inc=1, device_id=kv_id(y_at(d), my_x), device_id_type=MESH
        )
        pl.semaphore_signal(
            barrier, inc=1, device_id=kv_id(my_y, x_at(d)), device_id_type=MESH
        )
    pl.semaphore_wait(barrier, len(others) + 2 * (n_side - 1))

    tok_copy.wait()
    tok_sends = []
    for d, flip in reversed(others):
        to = tp_at(d, flip)
        cp = remote(
            tok_own, tok_all.at[me_t], tok_send_sem.at[to], tok_recv_sem.at[me_t], tp_id(to)
        )
        cp.start()
        tok_sends.append(cp)

    far_sends = []
    for j, src in enumerate(mats):
        for zz in range(n_z):
            cols = pl.ds(pl.multiple_of((2 * zz + 1 - my_c) * fpd, fpd), fpd)
            cp = remote(
                src.at[:, cols],
                far_w.at[j, zz],
                far_send_sem.at[j, zz],
                far_recv_sem.at[j, zz],
                tp_id(partner),
            )
            cp.start()
            far_sends.append(cp)

    zero_rows = jnp.zeros((upad - units, fpd), BF16)
    for cp in own_copies:
        cp.wait()
    for cp in far_sends:
        cp.wait_recv()
    for zz in range(n_z):
        cols = pl.ds(pl.multiple_of((2 * zz + my_c) * fpd, fpd), fpd)
        gain = mgain_ref[:, cols]
        here = slice(zz * fpd, (zz + 1) * fpd)
        for j in range(2):
            for s, src in enumerate((own_w, far_w)):
                row = (2 * j + s) * upad
                scaled = (src[j, zz].astype(F32) * gain).astype(BF16)
                gu[row : row + units, here] = scaled
                gu[row + units : row + upad, here] = zero_rows
        for s, src in enumerate((own_w, far_w)):
            wd[s * upad : s * upad + units, here] = src[2, zz]
            wd[s * upad + units : (s + 1) * upad, here] = zero_rows

    for cp in w_copies:
        cp.wait()
    acc = jnp.zeros((rows, 4 * head), F32)
    square = jnp.zeros((rows, fpd), F32)
    write_sum = jnp.zeros((rows, fpd), F32)
    decay_sum = jnp.zeros((rows, fpd), F32)
    for i, (d, flip) in enumerate([(0, 0)] + others):
        t = tp_at(d, flip)
        if i == 0:
            piece = tok_own[...].astype(F32)
        else:
            remote(
                tok_own, tok_all.at[t], tok_send_sem.at[t], tok_recv_sem.at[t], tp_id(t)
            ).wait_recv()
            piece = tok_all[t].astype(F32)
        cols = pl.ds(pl.multiple_of(t * fpd, fpd), fpd)
        square += piece * piece
        lhs = (piece * again_ref[:, cols]).astype(BF16)
        lhs32 = lhs.astype(F32)
        write_sum += lhs32 * wrates_ref[0:1, cols].astype(F32)
        decay_sum += lhs32 * wrates_ref[1:2, cols].astype(F32)
        acc += jnp.dot(lhs, wqkvg[cols, :], preferred_element_type=F32)
    count = fpd * n_tp
    scale = lax.rsqrt(jnp.sum(square, axis=1, keepdims=True) / count + EPS)
    acc = acc * scale
    query = acc[:, 0:head]
    key = acc[:, head : 2 * head]
    value = acc[:, 2 * head : 3 * head]
    gate_in = acc[:, 3 * head : 4 * head]
    write_raw = jnp.sum(write_sum, axis=1, keepdims=True) * scale
    decay_raw = jnp.sum(decay_sum, axis=1, keepdims=True) * scale
    unit_query = query * (
        lax.rsqrt(jnp.sum(query * query, axis=1, keepdims=True) + EPS) * head ** (-0.5)
    )
    unit_key = key * lax.rsqrt(jnp.sum(key * key, axis=1, keepdims=True) + EPS)
    strength = 1.0 / (1.0 + jnp.exp(-write_raw))
    softplus = jnp.maximum(decay_raw, 0.0) + jnp.log(1.0 + jnp.exp(-jnp.abs(decay_raw)))
    fade = jnp.exp(-hrate_ref[0] * softplus)

    state_copy.wait()
    stacked = jnp.concatenate(
        [unit_key, unit_query, jnp.zeros((head - 2 * rows, head), F32)], axis=0
    )
    turned = stacked.T
    for b in range(rows):
        block = state[b]
        pred[0, b : b + 1, :] = jnp.sum(turned[:, b : b + 1] * block, axis=0, keepdims=True)
        pred[1, b : b + 1, :] = jnp.sum(
            turned[:, rows + b : rows + b + 1] * block, axis=0, keepdims=True
        )
    fresh = strength * (value - fade * pred[0])
    overlap = jnp.sum(unit_query * unit_key, axis=1, keepdims=True)
    readout = fade * pred[1] + overlap * fresh
    normed_out = readout * lax.rsqrt(
        jnp.sum(readout * readout, axis=1, keepdims=True) / head + EPS
    )
    mixed = (
        normed_out * hgain_ref[...] * (gate_in / (1.0 + jnp.exp(-gate_in)))
    ).astype(BF16)

    wout_copy.wait()
    for t in range(n_tp):
        part1[t] = jnp.dot(
            mixed, wout[:, t * fpd : (t + 1) * fpd], preferred_element_type=F32
        ).astype(BF16)
    p1_sends = []
    for d, flip in reversed(others):
        to = tp_at(d, flip)
        cp = remote(
            part1.at[to], recv1.at[me_t], p1_send_sem.at[to], p1_recv_sem.at[me_t], tp_id(to)
        )
        cp.start()
        p1_sends.append(cp)

    for b in range(rows):
        ns[b] = fade[b : b + 1, :] * state[b] + turned[:, b : b + 1] * fresh[b : b + 1, :]
    ns_copy = pltpu.make_async_copy(ns, ns_hbm, local_sem.at[7])
    ns_copy.start()

    total = tok_own[...].astype(F32) + part1[me_t].astype(F32)
    for d, flip in others:
        t = tp_at(d, flip)
        remote(
            part1.at[t], recv1.at[t], p1_send_sem.at[t], p1_recv_sem.at[t], tp_id(t)
        ).wait_recv()
        total += recv1[t].astype(F32)
    residual = total.astype(BF16)
    ag[my_y, my_x, my_z] = residual

    agz_sends = []
    mine = ag.at[my_y, my_x, my_z]
    for d in reversed(near[1:]):
        zz = z_at(d)
        cp = remote(
            mine, mine, agz_send_sem.at[zz], agz_recv_sem.at[my_z], tp_id(zz * 2 + my_c)
        )
        cp.start()
        agz_sends.append(cp)
    for d in near[1:]:
        zz = z_at(d)
        slot = ag.at[my_y, my_x, zz]
        remote(
            slot, slot, agz_send_sem.at[zz], agz_recv_sem.at[zz], tp_id(zz * 2 + my_c)
        ).wait_recv()

    low, high = pl.ds(0, half), pl.ds(half, half)

    def spread(h, y, x, along_x, d, first=False):
        block = ag.at[y, x, (low, high)[h]]
        to = kv_id(my_y, x_at(d)) if along_x else kv_id(y_at(d), my_x)
        sent = ag_send_sem.at[2, h, 0, d] if first else ag_send_sem.at[h, y, x, d]
        return remote(block, block, sent, ag_recv_sem.at[h, y, x], to)

    def arrive(h, y, x):
        block = ag.at[y, x, (low, high)[h]]
        remote(
            block, block, ag_send_sem.at[h, y, x, 0], ag_recv_sem.at[h, y, x], kv_id(y, x)
        ).wait_recv()

    spread_order = [2, 1, 3] if n_side == 4 else list(range(1, n_side))
    arrive_order = [1, 3, 2] if n_side == 4 else list(range(1, n_side))
    ag_sends = []
    for d in spread_order:
        for h, along_x in ((0, True), (1, False)):
            cp = spread(h, my_y, my_x, along_x, d, first=True)
            cp.start()
            ag_sends.append(cp)
    for d in spread_order:
        for h, along_x in ((0, False), (1, True)):
            cp = spread(h, my_y, my_x, along_x, d)
            cp.start()
            ag_sends.append(cp)
    for d in arrive_order:
        arrive(0, my_y, x_at(d))
        for e in spread_order:
            cp = spread(0, my_y, x_at(d), False, e)
            cp.start()
            ag_sends.append(cp)
        arrive(1, y_at(d), my_x)
        for e in spread_order:
            cp = spread(1, y_at(d), my_x, True, e)
            cp.start()
            ag_sends.append(cp)
    for d in arrive_order:
        arrive(0, y_at(d), my_x)
        arrive(1, my_y, x_at(d))
    for d in arrive_order:
        for e in arrive_order:
            arrive(0, y_at(d), x_at(e))
            arrive(1, y_at(d), x_at(e))

    batch = rows * n_side * n_side
    acc2 = jnp.zeros((batch, 4 * upad), F32)
    sq2 = jnp.zeros((batch, 128), F32)
    for zz in range(n_z):
        lhs = ag[:, :, zz].reshape(batch, fpd)
        wide = lhs.astype(F32)
        wide = wide * wide
        for q in range(fpd // 128):
            sq2 += wide[:, q * 128 : (q + 1) * 128]
        acc2 += lax.dot_general(
            lhs,
            gu[:, zz * fpd : (zz + 1) * fpd],
            (((1,), (1,)), ((), ())),
            preferred_element_type=F32,
        )
    ex_out[0] = acc2[:, : 2 * upad]
    ex_out[1] = acc2[:, 2 * upad :]
    ex_out[2] = sq2
    ex_copy = remote(ex_out, ex_in, ex_send_sem, ex_recv_sem, tp_id(partner))
    ex_copy.start()
    ex_copy.wait_recv()
    row_scale = lax.rsqrt(
        jnp.sum(ex_out[2] + ex_in[2], axis=1, keepdims=True) / count + EPS
    )
    gate_far = pltpu.roll(ex_in[0], upad, 1)
    up_far = pltpu.roll(ex_in[1], upad, 1)
    gate_pre = (ex_out[0] + gate_far) * row_scale
    up_pre = (ex_out[1] + up_far) * row_scale
    hidden = (gate_pre / (1.0 + jnp.exp(-gate_pre)) * up_pre).astype(BF16)

    for zz in range(n_z):
        down = jnp.dot(hidden, wd[:, zz * fpd : (zz + 1) * fpd], preferred_element_type=F32)
        pb[:, :, zz] = down.astype(BF16).reshape(n_side, n_side, rows, fpd)
    r1_sends = []
    for d in spread_order:
        yy, xx = y_at(d), x_at(d)
        cp = remote(
            pb.at[yy, :, low], ra1.at[my_y], r1_send_sem.at[0, yy], r1_recv_sem.at[0, my_y],
            kv_id(yy, my_x),
        )
        cp.start()
        r1_sends.append(cp)
        cp = remote(
            pb.at[:, xx, high], rb1.at[my_x], r1_send_sem.at[1, xx], r1_recv_sem.at[1, my_x],
            kv_id(my_y, xx),
        )
        cp.start()
        r1_sends.append(cp)
    for d in arrive_order:
        yy, xx = y_at(d), x_at(d)
        remote(
            pb.at[yy, :, low], ra1.at[yy], r1_send_sem.at[0, yy], r1_recv_sem.at[0, yy],
            kv_id(yy, my_x),
        ).wait_recv()
        remote(
            pb.at[:, xx, high], rb1.at[xx], r1_send_sem.at[1, xx], r1_recv_sem.at[1, xx],
            kv_id(my_y, xx),
        ).wait_recv()
    r2_sends = []
    for e in spread_order + [0]:
        yy, xx = y_at(e), x_at(e)
        sum_a = pb[my_y, xx, 0:half].astype(F32)
        sum_b = pb[yy, my_x, half:n_z].astype(F32)
        for d in range(1, n_side):
            sum_a += ra1[y_at(d), xx].astype(F32)
            sum_b += rb1[x_at(d), yy].astype(F32)
        mid_a[xx] = sum_a.astype(BF16)
        mid_b[yy] = sum_b.astype(BF16)
        if e:
            cp = remote(
                mid_a.at[xx], ra2.at[my_x], r2_send_sem.at[0, xx], r2_recv_sem.at[0, my_x],
                kv_id(my_y, xx),
            )
            cp.start()
            r2_sends.append(cp)
            cp = remote(
                mid_b.at[yy], rb2.at[my_y], r2_send_sem.at[1, yy], r2_recv_sem.at[1, my_y],
                kv_id(yy, my_x),
            )
            cp.start()
            r2_sends.append(cp)
    sum_a = mid_a[my_x].astype(F32)
    sum_b = mid_b[my_y].astype(F32)
    for d in arrive_order:
        yy, xx = y_at(d), x_at(d)
        remote(
            mid_a.at[xx], ra2.at[xx], r2_send_sem.at[0, xx], r2_recv_sem.at[0, xx],
            kv_id(my_y, xx),
        ).wait_recv()
        sum_a += ra2[xx].astype(F32)
        remote(
            mid_b.at[yy], rb2.at[yy], r2_send_sem.at[1, yy], r2_recv_sem.at[1, yy],
            kv_id(yy, my_x),
        ).wait_recv()
        sum_b += rb2[yy].astype(F32)
    zout[0:half] = sum_a.astype(BF16)
    zout[half:n_z] = sum_b.astype(BF16)
    rz_sends = []
    for d in reversed(near[1:]):
        zz = z_at(d)
        cp = remote(
            zout.at[zz], zin.at[my_z], rz_send_sem.at[zz], rz_recv_sem.at[my_z],
            tp_id(zz * 2 + my_c),
        )
        cp.start()
        rz_sends.append(cp)
    out = residual.astype(F32) + zout[my_z].astype(F32)
    for d in near[1:]:
        zz = z_at(d)
        remote(
            zout.at[zz], zin.at[zz], rz_send_sem.at[zz], rz_recv_sem.at[zz],
            tp_id(zz * 2 + my_c),
        ).wait_recv()
        out += zin[zz].astype(F32)
    result_ref[...] = out.astype(BF16)

    ns_copy.wait()
    for cp in (
        tok_sends + far_sends + p1_sends + agz_sends + ag_sends + r1_sends + r2_sends + rz_sends
    ):
        cp.wait_send()
    ex_copy.wait_send()


def solution(mesh):
    n_kv, n_tp = mesh.shape["kv"], mesh.shape["tp"]
    n_side = math.isqrt(n_kv)
    n_z = n_tp // 2
    half = n_z // 2

    def body(
        tokens,
        attn_gain,
        w_query,
        w_key,
        w_value,
        w_outgate,
        w_rates,
        head_rate,
        head_gain,
        w_out,
        state,
        mlp_gain,
        w_gate,
        w_up,
        w_down,
    ):
        rows, fpd = tokens.shape
        feats = fpd * n_tp
        head = w_query.shape[1]
        units = w_gate.shape[1]
        upad = 64
        batch = rows * n_kv
        plane = fpd * n_z
        any_spec = pl.BlockSpec(memory_space=pl.ANY)
        vmem = pl.BlockSpec(memory_space=pltpu.VMEM)
        smem = pl.BlockSpec(memory_space=pltpu.SMEM)
        dma = pltpu.SemaphoreType.DMA

        def kernel(*refs):
            layer_kernel(n_side, n_z, *refs)

        result, new_state = pl.pallas_call(
            kernel,
            name="layer",
            out_shape=(
                jax.ShapeDtypeStruct((rows, fpd), BF16),
                jax.ShapeDtypeStruct((rows, head, head), F32),
            ),
            in_specs=[
                any_spec,
                vmem,
                any_spec,
                any_spec,
                any_spec,
                any_spec,
                vmem,
                smem,
                vmem,
                any_spec,
                any_spec,
                vmem,
                any_spec,
                any_spec,
                any_spec,
            ],
            out_specs=(vmem, any_spec),
            scratch_shapes=[
                pltpu.VMEM((rows, fpd), BF16),
                pltpu.VMEM((n_tp, rows, fpd), BF16),
                pltpu.VMEM((feats, 4 * head), BF16),
                pltpu.VMEM((head, feats), BF16),
                pltpu.VMEM((rows, head, head), F32),
                pltpu.VMEM((rows, head, head), F32),
                pltpu.VMEM((2, rows, head), F32),
                pltpu.VMEM((3, n_z, units, fpd), BF16),
                pltpu.VMEM((3, n_z, units, fpd), BF16),
                pltpu.VMEM((4 * upad, plane), BF16),
                pltpu.VMEM((2 * upad, plane), BF16),
                pltpu.VMEM((n_tp, rows, fpd), BF16),
                pltpu.VMEM((n_tp, rows, fpd), BF16),
                pltpu.VMEM((n_side, n_side, n_z, rows, fpd), BF16),
                pltpu.VMEM((3, batch, 128), F32),
                pltpu.VMEM((3, batch, 128), F32),
                pltpu.VMEM((n_side, n_side, n_z, rows, fpd), BF16),
                pltpu.VMEM((n_side, n_side, half, rows, fpd), BF16),
                pltpu.VMEM((n_side, half, rows, fpd), BF16),
                pltpu.VMEM((n_side, n_side, half, rows, fpd), BF16),
                pltpu.VMEM((n_side, half, rows, fpd), BF16),
                pltpu.VMEM((n_side, half, rows, fpd), BF16),
                pltpu.VMEM((n_side, half, rows, fpd), BF16),
                pltpu.VMEM((n_z, rows, fpd), BF16),
                pltpu.VMEM((n_z, rows, fpd), BF16),
                dma((8,)),
                dma((3, n_z)),
                dma((3, n_z)),
                dma((3, n_z)),
                dma((n_tp,)),
                dma((n_tp,)),
                dma((n_tp,)),
                dma((n_tp,)),
                dma((n_z,)),
                dma((n_z,)),
                dma((3, n_side, n_side, n_side)),
                dma((2, n_side, n_side)),
                dma,
                dma,
                dma((2, n_side)),
                dma((2, n_side)),
                dma((2, n_side)),
                dma((2, n_side)),
                dma((n_z,)),
                dma((n_z,)),
            ],
            compiler_params=pltpu.CompilerParams(
                collective_id=0,
                has_side_effects=True,
                vmem_limit_bytes=60 * 1024 * 1024,
            ),
        )(
            tokens,
            attn_gain.reshape(1, feats),
            w_query,
            w_key,
            w_value,
            w_outgate,
            w_rates.reshape(2, feats),
            head_rate,
            head_gain.reshape(1, head),
            w_out,
            state.reshape(rows, head, head),
            mlp_gain.reshape(1, feats),
            w_gate.T,
            w_up.T,
            w_down.T,
        )
        return result, new_state.reshape(rows, 1, head, head)

    return jax.shard_map(
        body,
        mesh=mesh,
        in_specs=(
            P("kv", "tp"),
            P(),
            P(None, "tp"),
            P(None, "tp"),
            P(None, "tp"),
            P(None, "tp"),
            P(None, None, "tp"),
            P("tp"),
            P("tp"),
            P("tp", None),
            P("kv", "tp", None, None),
            P(),
            P(None, ("kv", "tp")),
            P(None, ("kv", "tp")),
            P(None, ("kv", "tp")),
        ),
        out_specs=(P("kv", "tp"), P("kv", "tp", None, None)),
        check_vma=False,
    )
```

time: 157 us -> 65.6 us (0.42)
  blocking collectives: 81.7 us -> 0 us
  Pallas kernels: 0 us -> 60.4 us
  starting transfers between devices: 18.7 us -> 0 us
  waiting for transfers between devices: 18.5 us -> 0 us
  between operations: 15 us -> 1.29 us
  matrix products: 8.08 us -> 0 us
  local copies, waits for them, and re-layouts: 11.6 us -> 3.59 us
  other arithmetic: 2.96 us -> 0 us
    all_to_all x4 -> x0, blocking collectives: 81.7 us -> none  [the longest x2 61.2 us: copy_for_each(): lax.all_to_all(jnp.broadcast_to(value[None], (size, *value.shape)), axis,...]
    pallas_call x0 -> x1, Pallas kernels: none -> 60.4 us  [body(): pl.pallas_call(kernel, name='layer', out_shape=(jax.ShapeDtypeStruct((row...]
    all_to_all x2 -> x0, starting transfers between devices: 18.7 us -> none  [the longest x1 9.97 us: copy_for_each(): lax.all_to_all(jnp.broadcast_to(value[None], (size, *value.shape)), axis,...]
    all_to_all x2 -> x0, waiting for transfers between devices: 17.8 us -> none  [the longest x1 10.3 us: sent_and_summed_2(): lax.all_to_all(tiles, axis, split_axis=0, concat_axis=0, tiled=True)]
    dot_general x10 -> x0, matrix products: 8.08 us -> none  [the longest x1 4.19 us: down_product(): lax.dot_general(hidden, down_part, (((1,), (1,)), ((), ())), preferred_el...]
    unnamed x29 -> x2, local copies, waits for them, and re-layouts: 8.94 us -> 3.59 us
    broadcast_in_dim x3 -> x0, local copies, waits for them, and re-layouts: 1.6 us -> none  [copy_for_each(): jnp.broadcast_to(value[None], (size, *value.shape))]
  transfers between devices with their start and end apart: 3 -> 0, of which waited for: 2 -> 0; matrix products, arithmetic and copies ran while one was open for 6% -> 0% of each run, Pallas kernels for 0% -> 0%
where the time goes in v1:
time: 65.6 us; the launch traced here: 65.3 us
  Pallas kernels  60.4 us (92%)
  local copies, waits for them, and re-layouts  3.59 us (5%)
  between operations  1.29 us (2%)
    pallas_call x1, Pallas kernels, body(): pl.pallas_call(kernel, name='layer', out_shape=(jax.ShapeDtypeStruct((row...  60.4 us
    unnamed x2, local copies, waits for them, and re-layouts  3.59 us

profile of v1, /device:TPU:1, one launch (start us, length us, event | category | flops | bytes accessed | tf_op | source)
XLA Modules:
  0.0 65.3 jit_solution(15638757454070401416)
XLA Ops:
  1.3 60.4 %layer.1 = (bf16[16,256]{1,0:T(8,128)(2,1)}, f32[16,128,128]{2,1,0:T(8,128)}) custom-call(bf16[16,256]{1,0:T(8,128)(2,1)} %refs_0_.1, f32[1,4096]{1,0:T(1,128)} %bitcast.16, bf16[4096,128]{1,0:T(8,128)(2,1)} %refs_2_.1, bf16[4096,128]{1,0:T(8,128)(2,1)} %refs_3_.1, bf16[4096,128]{1,0:T(8,128)(2,1)} %refs_4_.1, bf16[4096,128]{1,0:T(8,128)(2,1)} %refs_5_.1, ...), custom_call_target="tpu_custom_call" | custom-call | tf_op jit(solution)/shard_map/layer/pallas_call | solution.py:521
  61.7 1.3 %copy.21 = bf16[16,256]{1,0:T(8,128)(2,1)} copy(bf16[16,256]{1,0:T(8,128)(2,1)} %get-tuple-element.10) | data formatting | bytes 16384
  63.0 2.3 %copy.22 = f32[16,1,128,128]{3,2,1,0:T(8,128)} copy(f32[16,1,128,128]{3,2,1,0:T(8,128)} %bitcast.12) | data formatting | bytes 2097152

commit v2 on v0

v2 whole, which is shorter than its diff:
```python
import math

import jax
import jax.numpy as jnp
from jax import lax
from jax.experimental import pallas as pl
from jax.experimental.pallas import tpu as pltpu
from jax.sharding import PartitionSpec as P

EPS = 1e-06
MESH = pl.DeviceIdType.MESH
F32 = jnp.float32
BF16 = jnp.bfloat16


def layer_kernel(
    n_side,
    n_z,
    tok_hbm,
    again_hbm,
    wq_hbm,
    wk_hbm,
    wv_hbm,
    wo_hbm,
    wrates_hbm,
    hrate_ref,
    hgain_hbm,
    wout_hbm,
    state_hbm,
    mgain_hbm,
    wgate_hbm,
    wup_hbm,
    wdown_hbm,
    result_out,
    ns_out,
    tok_own,
    tok_all,
    wqkvg,
    wout,
    state,
    pred,
    again,
    mgain,
    hgain,
    wrates,
    own_w,
    far_w,
    gu,
    wd,
    part1,
    recv1,
    ag,
    ex_out,
    ex_in,
    exsq_out,
    exsq_in,
    pb,
    r1,
    mid,
    r2,
    zout,
    zin,
    local_sem,
    far_send_sem,
    far_recv_sem,
    tok_send_sem,
    tok_recv_sem,
    p1_send_sem,
    p1_recv_sem,
    agz_send_sem,
    agz_recv_sem,
    ag_send_sem,
    ag_recv_sem,
    ex_send_sem,
    ex_recv_sem,
    r_send_sem,
    r_recv_sem,
    rz_send_sem,
    rz_recv_sem,
):
    n_tp = 2 * n_z
    rows, fpd = tok_own.shape
    head = hgain.shape[1]
    units = own_w.shape[1]
    upad = gu.shape[1] // 4
    me_k = lax.axis_index("kv")
    me_t = lax.axis_index("tp")
    my_y, my_x = me_k // n_side, lax.rem(me_k, n_side)
    my_z, my_c = me_t // 2, lax.rem(me_t, 2)
    partner = me_t + 1 - 2 * my_c

    def z_at(d):
        return lax.rem(my_z + d, n_z)

    def y_at(d):
        return lax.rem(my_y + d, n_side)

    def x_at(d):
        return lax.rem(my_x + d, n_side)

    def tp_id(t):
        return {"tp": t}

    def kv_id(y, x):
        return {"kv": y * n_side + x}

    def local(src, dst, sem):
        cp = pltpu.make_async_copy(src, dst, sem)
        cp.start()
        return cp

    def send(src, dst, sent, received, device):
        pltpu.make_async_remote_copy(
            src_ref=src,
            dst_ref=dst,
            send_sem=sent,
            recv_sem=received,
            device_id=device,
            device_id_type=MESH,
        ).start()

    def await_bytes(like, sem):
        pltpu.make_async_copy(like, like, sem).wait()

    near = [0]
    for d in range(1, n_z // 2):
        near += [d, n_z - d]
    near += [n_z // 2]
    others = [(d, flip) for d in near for flip in (0, 1)][1:]
    side_far = [2, 1, 3] if n_side == 4 else list(range(1, n_side))
    side_near = side_far[1:] + side_far[:1]

    def tp_at(d, flip):
        c = (1 - my_c) if flip else my_c
        return z_at(d) * 2 + c

    def group_of(d):
        return 0 if min(d, n_z - d) <= 1 else (1 if min(d, n_z - d) == 2 else 2)

    tok_copy = local(tok_hbm, tok_own, local_sem.at[0])
    small = [
        local(again_hbm, again, local_sem.at[1]),
        local(mgain_hbm, mgain, local_sem.at[2]),
        local(hgain_hbm, hgain, local_sem.at[3]),
        local(wrates_hbm, wrates, local_sem.at[4]),
    ]
    mats = (wgate_hbm, wup_hbm, wdown_hbm)
    own_copies = [local(src, own_w.at[j], local_sem.at[5 + j]) for j, src in enumerate(mats)]
    w_copies = [
        local(src, wqkvg.at[:, pl.ds(j * head, head)], local_sem.at[8 + j])
        for j, src in enumerate((wq_hbm, wk_hbm, wv_hbm, wo_hbm))
    ]
    state_copy = local(state_hbm, state, local_sem.at[12])
    wout_copy = local(wout_hbm, wout, local_sem.at[13])

    barrier = pltpu.get_barrier_semaphore()
    for d, flip in reversed(others):
        pl.semaphore_signal(
            barrier, inc=1, device_id=tp_id(tp_at(d, flip)), device_id_type=MESH
        )
    for d in range(1, n_side):
        pl.semaphore_signal(
            barrier, inc=1, device_id=kv_id(y_at(d), my_x), device_id_type=MESH
        )
        pl.semaphore_signal(
            barrier, inc=1, device_id=kv_id(my_y, x_at(d)), device_id_type=MESH
        )
    tok_copy.wait()
    pl.semaphore_wait(barrier, len(others) + 2 * (n_side - 1))

    for d, flip in reversed(others):
        send(
            tok_own,
            tok_all.at[me_t],
            tok_send_sem,
            tok_recv_sem.at[group_of(d)],
            tp_id(tp_at(d, flip)),
        )

    for j, src in enumerate(mats):
        send(src, far_w.at[j], far_send_sem.at[j], far_recv_sem.at[j], tp_id(partner))

    for cp in small + w_copies:
        cp.wait()
    acc = jnp.zeros((rows, 4 * head), F32)
    square = jnp.zeros((rows, fpd), F32)
    write_sum = jnp.zeros((rows, fpd), F32)
    decay_sum = jnp.zeros((rows, fpd), F32)
    seen = set()
    for i, (d, flip) in enumerate([(0, 0)] + others):
        t = tp_at(d, flip)
        if i == 0:
            piece = tok_own[...].astype(F32)
        else:
            g = group_of(d)
            if g not in seen:
                seen.add(g)
                size = sum(group_of(e) == g for e, _ in others)
                await_bytes(tok_all.at[pl.ds(0, size)], tok_recv_sem.at[g])
            piece = tok_all[t].astype(F32)
        cols = pl.ds(pl.multiple_of(t * fpd, fpd), fpd)
        square += piece * piece
        lhs = (piece * again[:, cols]).astype(BF16)
        lhs32 = lhs.astype(F32)
        write_sum += lhs32 * wrates[0:1, cols].astype(F32)
        decay_sum += lhs32 * wrates[1:2, cols].astype(F32)
        acc += jnp.dot(lhs, wqkvg[cols, :], preferred_element_type=F32)
    count = fpd * n_tp
    scale = lax.rsqrt(jnp.sum(square, axis=1, keepdims=True) / count + EPS)
    acc = acc * scale
    query = acc[:, 0:head]
    key = acc[:, head : 2 * head]
    value = acc[:, 2 * head : 3 * head]
    gate_in = acc[:, 3 * head : 4 * head]
    write_raw = jnp.sum(write_sum, axis=1, keepdims=True) * scale
    decay_raw = jnp.sum(decay_sum, axis=1, keepdims=True) * scale
    unit_query = query * (
        lax.rsqrt(jnp.sum(query * query, axis=1, keepdims=True) + EPS) * head ** (-0.5)
    )
    unit_key = key * lax.rsqrt(jnp.sum(key * key, axis=1, keepdims=True) + EPS)
    strength = 1.0 / (1.0 + jnp.exp(-write_raw))
    softplus = jnp.maximum(decay_raw, 0.0) + jnp.log(1.0 + jnp.exp(-jnp.abs(decay_raw)))
    fade = jnp.exp(-hrate_ref[0] * softplus)

    state_copy.wait()
    stacked = jnp.concatenate(
        [unit_key, unit_query, jnp.zeros((head - 2 * rows, head), F32)], axis=0
    )
    turned = stacked.T
    for b in range(rows):
        block = state[b]
        pred[0, b : b + 1, :] = jnp.sum(turned[:, b : b + 1] * block, axis=0, keepdims=True)
        pred[1, b : b + 1, :] = jnp.sum(
            turned[:, rows + b : rows + b + 1] * block, axis=0, keepdims=True
        )
    fresh = strength * (value - fade * pred[0])
    overlap = jnp.sum(unit_query * unit_key, axis=1, keepdims=True)
    readout = fade * pred[1] + overlap * fresh
    normed_out = readout * lax.rsqrt(
        jnp.sum(readout * readout, axis=1, keepdims=True) / head + EPS
    )
    mixed = (normed_out * hgain[...] * (gate_in / (1.0 + jnp.exp(-gate_in)))).astype(BF16)

    wout_copy.wait()
    partial = jnp.dot(mixed, wout[...], preferred_element_type=F32).astype(BF16)
    for t in range(n_tp):
        part1[t] = partial[:, t * fpd : (t + 1) * fpd]
    for d, flip in reversed(others):
        to = tp_at(d, flip)
        send(part1.at[to], recv1.at[me_t], p1_send_sem, p1_recv_sem, tp_id(to))

    for b in range(rows):
        ns_out[b] = fade[b : b + 1, :] * state[b] + turned[:, b : b + 1] * fresh[b : b + 1, :]

    for cp in own_copies:
        cp.wait()
    for j in range(3):
        await_bytes(far_w.at[j], far_recv_sem.at[j])
    zero_rows = jnp.zeros((upad - units, fpd), BF16)
    for zz in range(n_z):
        cols = pl.ds(pl.multiple_of((2 * zz + my_c) * fpd, fpd), fpd)
        gain = mgain[:, cols]
        for s, src in enumerate((own_w, far_w)):
            for j in range(2):
                row = (2 * j + s) * upad
                scaled = (src[j, :, cols].astype(F32) * gain).astype(BF16)
                gu[zz, row : row + units, :] = scaled
                gu[zz, row + units : row + upad, :] = zero_rows
            wd[zz, s * upad : s * upad + units, :] = src[2, :, cols]
            wd[zz, s * upad + units : (s + 1) * upad, :] = zero_rows

    total = tok_own[...].astype(F32) + part1[me_t].astype(F32)
    await_bytes(recv1.at[pl.ds(0, n_tp - 1)], p1_recv_sem)
    for d, flip in others:
        total += recv1[tp_at(d, flip)].astype(F32)
    residual = total.astype(BF16)
    ag[my_z, my_y, my_x] = residual

    mine = ag.at[my_z, my_y, my_x]
    for d in reversed(near[1:]):
        back = (n_z - d) % n_z
        send(mine, mine, agz_send_sem, agz_recv_sem.at[back], tp_id(z_at(d) * 2 + my_c))

    def x_first(d):
        return near.index(d) % 2 == 0

    def first_to(d, e):
        return kv_id(my_y, x_at(e)) if x_first(d) else kv_id(y_at(e), my_x)

    def second_to(d, e):
        return kv_id(y_at(e), my_x) if x_first(d) else kv_id(my_y, x_at(e))

    def spread_own(d):
        block = ag.at[z_at(d), my_y, my_x]
        if d:
            await_bytes(block, agz_recv_sem.at[d])
        for e in side_far:
            send(block, block, ag_send_sem.at[0], ag_recv_sem.at[0, d], first_to(d, e))
        for e in side_far:
            send(block, block, ag_send_sem.at[1], ag_recv_sem.at[1, d], second_to(d, e))

    def spread_on(d):
        z = z_at(d)
        await_bytes(ag.at[z, 0, pl.ds(0, n_side - 1)], ag_recv_sem.at[0, d])
        for e in side_far:
            for f in side_near:
                block = ag.at[z, my_y, x_at(f)] if x_first(d) else ag.at[z, y_at(f), my_x]
                send(block, block, ag_send_sem.at[1], ag_recv_sem.at[1, d], second_to(d, e))

    batch = rows * n_side * n_side
    sums = [jnp.zeros((batch, 4 * upad), F32), jnp.zeros((batch, 128), F32)]

    def multiply(d):
        z = z_at(d)
        await_bytes(ag.at[z, pl.ds(0, n_side - 1)], ag_recv_sem.at[1, d])
        lhs = ag[z].reshape(batch, fpd)
        wide = lhs.astype(F32)
        wide = wide * wide
        for q in range(fpd // 128):
            sums[1] += wide[:, q * 128 : (q + 1) * 128]
        sums[0] += lax.dot_general(
            lhs, gu[z], (((1,), (1,)), ((), ())), preferred_element_type=F32
        )

    steps = (
        [(0, i) for i in range(3)]
        + [(1, 0)]
        + [(0, i) for i in range(3, n_z)]
        + [(1, i) for i in range(1, n_z)]
        + [(2, i) for i in range(n_z)]
    )
    for what, i in steps:
        (spread_own, spread_on, multiply)[what](near[i])

    ex_out[0] = sums[0][:, : 2 * upad].astype(BF16)
    ex_out[1] = sums[0][:, 2 * upad :].astype(BF16)
    exsq_out[...] = sums[1]
    send(ex_out, ex_in, ex_send_sem.at[0], ex_recv_sem.at[0], tp_id(partner))
    send(exsq_out, exsq_in, ex_send_sem.at[1], ex_recv_sem.at[1], tp_id(partner))
    await_bytes(ex_in, ex_recv_sem.at[0])
    await_bytes(exsq_in, ex_recv_sem.at[1])
    row_scale = lax.rsqrt(
        jnp.sum(sums[1] + exsq_in[...], axis=1, keepdims=True) / count + EPS
    )
    gate_far = pltpu.roll(ex_in[0].astype(F32), upad, 1)
    up_far = pltpu.roll(ex_in[1].astype(F32), upad, 1)
    gate_pre = (sums[0][:, : 2 * upad] + gate_far) * row_scale
    up_pre = (sums[0][:, 2 * upad :] + up_far) * row_scale
    hidden = (gate_pre / (1.0 + jnp.exp(-gate_pre)) * up_pre).astype(BF16)

    def send_first(d):
        z = z_at(d)
        for e in side_far:
            for f in side_near:
                if x_first(d):
                    block, slot, at = pb.at[z, y_at(e), x_at(f)], my_y, x_at(f)
                else:
                    block, slot, at = pb.at[z, y_at(f), x_at(e)], my_x, y_at(f)
                send(
                    block, r1.at[z, slot, at], r_send_sem.at[0], r_recv_sem.at[0, d],
                    second_to(d, e),
                )

    def sum_first(d):
        z = z_at(d)
        await_bytes(
            r1.at[z, pl.ds(0, n_side - 1), pl.ds(0, n_side - 1)], r_recv_sem.at[0, d]
        )
        for f in side_far:
            if x_first(d):
                block, place, at = pb[z, my_y, x_at(f)], y_at, x_at(f)
            else:
                block, place, at = pb[z, y_at(f), my_x], x_at, y_at(f)
            block = block.astype(F32)
            for e in side_near:
                block += r1[z, place(e), at].astype(F32)
            mid[z, at] = block.astype(BF16)

    def send_second(d):
        z = z_at(d)
        for e in side_far:
            at, slot = (x_at(e), my_x) if x_first(d) else (y_at(e), my_y)
            send(
                mid.at[z, at], r2.at[z, slot], r_send_sem.at[1], r_recv_sem.at[1, d],
                first_to(d, e),
            )
        for e in side_far:
            if x_first(d):
                block, slot = pb.at[z, y_at(e), my_x], r1.at[z, my_y, my_x]
            else:
                block, slot = pb.at[z, my_y, x_at(e)], r1.at[z, my_x, my_y]
            send(block, slot, r_send_sem.at[0], r_recv_sem.at[2, d], second_to(d, e))

    def sum_second(d):
        z = z_at(d)
        await_bytes(r2.at[z, pl.ds(0, n_side - 1)], r_recv_sem.at[1, d])
        await_bytes(r1.at[z, 0, pl.ds(0, n_side - 1)], r_recv_sem.at[2, d])
        first, me_first, second = (x_at, my_x, y_at) if x_first(d) else (y_at, my_y, x_at)
        block = pb[z, my_y, my_x].astype(F32)
        for e in side_near:
            block += r1[z, second(e), me_first].astype(F32)
        for e in side_near:
            block += r2[z, first(e)].astype(F32)
        zout[z] = block.astype(BF16)

    def send_third(d):
        if d:
            send(
                zout.at[z_at(d)], zin.at[my_z], rz_send_sem, rz_recv_sem,
                tp_id(z_at(d) * 2 + my_c),
            )

    far = list(reversed(near))
    for i, d in enumerate(far):
        z = z_at(d)
        down = jnp.dot(hidden, wd[z], preferred_element_type=F32)
        pb[z] = down.astype(BF16).reshape(n_side, n_side, rows, fpd)
        if i:
            send_first(far[i - 1])
    send_first(far[-1])
    lag = 4
    for i in range(n_z + lag + 1):
        if i < n_z:
            sum_first(far[i])
        if 0 <= i - 1 < n_z:
            send_second(far[i - 1])
        if 0 <= i - lag < n_z:
            sum_second(far[i - lag])
        if 0 <= i - lag - 1 < n_z:
            send_third(far[i - lag - 1])
    out = residual.astype(F32) + zout[my_z].astype(F32)
    await_bytes(zin.at[pl.ds(0, n_z - 1)], rz_recv_sem)
    for d in near[1:]:
        out += zin[z_at(d)].astype(F32)
    result_out[...] = out.astype(BF16)

    await_bytes(tok_all.at[pl.ds(0, n_tp - 1)], tok_send_sem)
    for j in range(3):
        await_bytes(far_w.at[j], far_send_sem.at[j])
    await_bytes(recv1.at[pl.ds(0, n_tp - 1)], p1_send_sem)
    await_bytes(zin.at[pl.ds(0, n_z - 1)], agz_send_sem)
    await_bytes(ag.at[:, 0, pl.ds(0, n_side - 1)], ag_send_sem.at[0])
    await_bytes(ag.at[:, pl.ds(0, n_side - 1)], ag_send_sem.at[1])
    await_bytes(ex_in, ex_send_sem.at[0])
    await_bytes(exsq_in, ex_send_sem.at[1])
    await_bytes(ag.at[:, pl.ds(0, n_side - 1)], r_send_sem.at[0])
    await_bytes(ag.at[:, 0, pl.ds(0, n_side - 1)], r_send_sem.at[1])
    await_bytes(zin.at[pl.ds(0, n_z - 1)], rz_send_sem)


def write_kernel(result_ref, ns_ref, result_out, ns_out, sem):
    copies = [
        pltpu.make_async_copy(ns_ref, ns_out, sem.at[0]),
        pltpu.make_async_copy(result_ref, result_out, sem.at[1]),
    ]
    for cp in copies:
        cp.start()
    for cp in copies:
        cp.wait()


def solution(mesh):
    n_kv, n_tp = mesh.shape["kv"], mesh.shape["tp"]
    n_side = math.isqrt(n_kv)
    n_z = n_tp // 2

    def body(
        tokens,
        attn_gain,
        w_query,
        w_key,
        w_value,
        w_outgate,
        w_rates,
        head_rate,
        head_gain,
        w_out,
        state,
        mlp_gain,
        w_gate,
        w_up,
        w_down,
    ):
        rows, fpd = tokens.shape
        feats = fpd * n_tp
        head = w_query.shape[1]
        units = w_gate.shape[1]
        upad = 64
        batch = rows * n_kv
        hbm = pl.BlockSpec(memory_space=pl.ANY)
        out_hbm = pl.BlockSpec(memory_space=pltpu.VMEM)
        smem = pl.BlockSpec(memory_space=pltpu.SMEM)
        dma = pltpu.SemaphoreType.DMA
        vmem = pltpu.VMEM

        def kernel(*refs):
            layer_kernel(n_side, n_z, *refs)

        operands = (
            tokens,
            attn_gain.reshape(1, feats),
            w_query,
            w_key,
            w_value,
            w_outgate,
            w_rates.reshape(2, feats),
            head_rate,
            head_gain.reshape(1, head),
            w_out,
            state.reshape(rows, head, head),
            mlp_gain.reshape(1, feats),
            w_gate.T,
            w_up.T,
            w_down.T,
        )
        operands = [
            a if a is head_rate else pltpu.with_memory_space_constraint(a, pltpu.HBM)
            for a in operands
        ]
        result, new_state = pl.pallas_call(
            kernel,
            name="layer",
            out_shape=(
                jax.ShapeDtypeStruct((rows, fpd), BF16),
                jax.ShapeDtypeStruct((rows, head, head), F32),
            ),
            in_specs=[hbm] * 7 + [smem] + [hbm] * 7,
            out_specs=(out_hbm, out_hbm),
            scratch_shapes=[
                vmem((rows, fpd), BF16),
                vmem((n_tp, rows, fpd), BF16),
                vmem((feats, 4 * head), BF16),
                vmem((head, feats), BF16),
                vmem((rows, head, head), F32),
                vmem((2, rows, head), F32),
                vmem((1, feats), F32),
                vmem((1, feats), F32),
                vmem((1, head), F32),
                vmem((2, feats), BF16),
                vmem((3, units, feats), BF16),
                vmem((3, units, feats), BF16),
                vmem((n_z, 4 * upad, fpd), BF16),
                vmem((n_z, 2 * upad, fpd), BF16),
                vmem((n_tp, rows, fpd), BF16),
                vmem((n_tp, rows, fpd), BF16),
                vmem((n_z, n_side, n_side, rows, fpd), BF16),
                vmem((2, batch, 2 * upad), BF16),
                vmem((2, batch, 2 * upad), BF16),
                vmem((batch, 128), F32),
                vmem((batch, 128), F32),
                vmem((n_z, n_side, n_side, rows, fpd), BF16),
                vmem((n_z, n_side, n_side, rows, fpd), BF16),
                vmem((n_z, n_side, rows, fpd), BF16),
                vmem((n_z, n_side, rows, fpd), BF16),
                vmem((n_z, rows, fpd), BF16),
                vmem((n_z, rows, fpd), BF16),
                dma((14,)),
                dma((3,)),
                dma((3,)),
                dma,
                dma((3,)),
                dma,
                dma,
                dma,
                dma((n_z,)),
                dma((2,)),
                dma((2, n_z)),
                dma((2,)),
                dma((2,)),
                dma((2,)),
                dma((3, n_z)),
                dma,
                dma,
            ],
            compiler_params=pltpu.CompilerParams(
                collective_id=0,
                has_side_effects=True,
                vmem_limit_bytes=50000 * 1024,
            ),
        )(*operands)
        result, new_state = pl.pallas_call(
            write_kernel,
            name="write",
            out_shape=(
                jax.ShapeDtypeStruct((rows, fpd), BF16),
                jax.ShapeDtypeStruct((rows, head, head), F32),
            ),
            in_specs=[pl.BlockSpec(memory_space=pltpu.VMEM)] * 2,
            out_specs=(pl.BlockSpec(memory_space=pl.ANY),) * 2,
            scratch_shapes=[dma((2,))],
            compiler_params=pltpu.CompilerParams(vmem_limit_bytes=4096 * 1024),
        )(result, new_state)
        return result, new_state.reshape(rows, 1, head, head)

    return jax.shard_map(
        body,
        mesh=mesh,
        in_specs=(
            P("kv", "tp"),
            P(),
            P(None, "tp"),
            P(None, "tp"),
            P(None, "tp"),
            P(None, "tp"),
            P(None, None, "tp"),
            P("tp"),
            P("tp"),
            P("tp", None),
            P("kv", "tp", None, None),
            P(),
            P(None, ("kv", "tp")),
            P(None, ("kv", "tp")),
            P(None, ("kv", "tp")),
        ),
        out_specs=(P("kv", "tp"), P("kv", "tp", None, None)),
        check_vma=False,
    )
```

time: 157 us -> 56 us (0.36)
  blocking collectives: 81.7 us -> 0 us
  Pallas kernels: 0 us -> 54.5 us
  starting transfers between devices: 18.7 us -> 0 us
  waiting for transfers between devices: 18.5 us -> 0 us
  between operations: 15 us -> 1.29 us
  local copies, waits for them, and re-layouts: 11.6 us -> 0 us
  matrix products: 8.08 us -> 0 us
  other arithmetic: 2.96 us -> 0 us
    all_to_all x4 -> x0, blocking collectives: 81.7 us -> none  [the longest x2 61.2 us: copy_for_each(): lax.all_to_all(jnp.broadcast_to(value[None], (size, *value.shape)), axis,...]
    pallas_call x0 -> x2, Pallas kernels: none -> 54.5 us  [the longest x1 53.5 us: body(): pl.pallas_call(kernel, name='layer', out_shape=(jax.ShapeDtypeStruct((row...]
    all_to_all x2 -> x0, starting transfers between devices: 18.7 us -> none  [the longest x1 9.97 us: copy_for_each(): lax.all_to_all(jnp.broadcast_to(value[None], (size, *value.shape)), axis,...]
    all_to_all x2 -> x0, waiting for transfers between devices: 17.8 us -> none  [the longest x1 10.3 us: sent_and_summed_2(): lax.all_to_all(tiles, axis, split_axis=0, concat_axis=0, tiled=True)]
    unnamed x29 -> x0, local copies, waits for them, and re-layouts: 8.94 us -> none
    dot_general x10 -> x0, matrix products: 8.08 us -> none  [the longest x1 4.19 us: down_product(): lax.dot_general(hidden, down_part, (((1,), (1,)), ((), ())), preferred_el...]
    broadcast_in_dim x3 -> x0, local copies, waits for them, and re-layouts: 1.6 us -> none  [copy_for_each(): jnp.broadcast_to(value[None], (size, *value.shape))]
  transfers between devices with their start and end apart: 3 -> 0, of which waited for: 2 -> 0; matrix products, arithmetic and copies ran while one was open for 6% -> 0% of each run, Pallas kernels for 0% -> 0%
where the time goes in v2:
time: 56 us; the launch traced here: 55.8 us
  Pallas kernels  54.5 us (97%)
  between operations  1.29 us (2%)
    pallas_call x1, Pallas kernels, body(): pl.pallas_call(kernel, name='layer', out_shape=(jax.ShapeDtypeStruct((row...  53.5 us

profile of v2, /device:TPU:1, one launch (start us, length us, event | category | flops | bytes accessed | tf_op | source)
XLA Modules:
  0.0 55.8 jit_solution(12141754239172579586)
XLA Ops:
  1.3 53.5 %layer.1 = (bf16[16,256]{1,0:T(8,128)(2,1)S(1)}, f32[16,128,128]{2,1,0:T(8,128)S(1)}) custom-call(bf16[16,256]{1,0:T(8,128)(2,1)} %refs_0_.1, f32[1,4096]{1,0:T(1,128)} %bitcast.15, bf16[4096,128]{1,0:T(8,128)(2,1)} %refs_2_.1, bf16[4096,128]{1,0:T(8,128)(2,1)} %refs_3_.1, bf16[4096,128]{1,0:T(8,128)(2,1)} %refs_4_.1, bf16[4096,128]{1,0:T(8,128)(2,1)} %refs_5_.1, ...), custom_call_target="tpu_custom_call" | custom-call | tf_op jit(solution)/shard_map/layer/pallas_call | solution.py:520
  54.8 1.0 %write.1 = (bf16[16,256]{1,0:T(8,128)(2,1)}, f32[16,128,128]{2,1,0:T(8,128)}) custom-call(bf16[16,256]{1,0:T(8,128)(2,1)S(1)} %get-tuple-element.6.result_ref, f32[16,128,128]{2,1,0:T(8,128)S(1)} %get-tuple-element.7.ns_ref), custom_call_target="tpu_custom_call" | custom-call | tf_op jit(solution)/shard_map/write/pallas_call | solution.py:581

commit v3 on v2

--- a/solution.py
+++ b/solution.py
@@ -13,9 +13,37 @@
 BF16 = jnp.bfloat16
 
 
+def schedule(n_z, parts):
+    every = range(n_z)
+    steps = [("own", h, i) for i in range(3) for h in range(parts)]
+    steps += [("on", h, 0) for h in range(parts)]
+    steps += [("own", h, i) for i in range(3, n_z) for h in range(parts)]
+    steps += [("on", h, i) for i in range(1, n_z) for h in range(parts)]
+    for h in range(parts):
+        steps += [("mm", h, i) for i in every] + [("swap", h), ("act", h)]
+        for i in every:
+            steps.append(("down", h, i))
+            if i:
+                steps.append(("s1", h, i - 1))
+        steps.append(("s1", h, n_z - 1))
+    lag = 8
+    for h in range(parts):
+        for i in range(n_z + lag + 1):
+            if i < n_z:
+                steps.append(("a1", h, i))
+            if 0 <= i - 1 < n_z:
+                steps.append(("s2", h, i - 1))
+            if 0 <= i - lag < n_z:
+                steps.append(("a2", h, i - lag))
+            if 0 <= i - lag - 1 < n_z:
+                steps.append(("s3", h, i - lag - 1))
+    return steps
+
+
 def layer_kernel(
     n_side,
     n_z,
+    parts,
     tok_hbm,
     again_hbm,
     wq_hbm,
@@ -23,7 +51,7 @@
     wv_hbm,
     wo_hbm,
     wrates_hbm,
-    hrate_ref,
+    hrate_hbm,
     hgain_hbm,
     wout_hbm,
     state_hbm,
@@ -42,6 +70,7 @@
     again,
     mgain,
     hgain,
+    hrate,
     wrates,
     own_w,
     far_w,
@@ -79,6 +108,7 @@
     rz_recv_sem,
 ):
     n_tp = 2 * n_z
+    sub = ag.shape[4]
     rows, fpd = tok_own.shape
     head = hgain.shape[1]
     units = own_w.shape[1]
@@ -135,7 +165,7 @@
         return z_at(d) * 2 + c
 
     def group_of(d):
-        return 0 if min(d, n_z - d) <= 1 else (1 if min(d, n_z - d) == 2 else 2)
+        return max(min(d, n_z - d) - 1, 0)
 
     tok_copy = local(tok_hbm, tok_own, local_sem.at[0])
     small = [
@@ -143,6 +173,7 @@
         local(mgain_hbm, mgain, local_sem.at[2]),
         local(hgain_hbm, hgain, local_sem.at[3]),
         local(wrates_hbm, wrates, local_sem.at[4]),
+        local(hrate_hbm, hrate, local_sem.at[14]),
     ]
     mats = (wgate_hbm, wup_hbm, wdown_hbm)
     own_copies = [local(src, own_w.at[j], local_sem.at[5 + j]) for j, src in enumerate(mats)]
@@ -220,7 +251,7 @@
     unit_key = key * lax.rsqrt(jnp.sum(key * key, axis=1, keepdims=True) + EPS)
     strength = 1.0 / (1.0 + jnp.exp(-write_raw))
     softplus = jnp.maximum(decay_raw, 0.0) + jnp.log(1.0 + jnp.exp(-jnp.abs(decay_raw)))
-    fade = jnp.exp(-hrate_ref[0] * softplus)
+    fade = jnp.exp(-hrate[:, 0:1] * softplus)
 
     state_copy.wait()
     stacked = jnp.concatenate(
@@ -274,9 +305,10 @@
     for d, flip in others:
         total += recv1[tp_at(d, flip)].astype(F32)
     residual = total.astype(BF16)
-    ag[my_z, my_y, my_x] = residual
-
-    mine = ag.at[my_z, my_y, my_x]
+    for h in range(parts):
+        ag[h, my_z, my_y, my_x] = residual[h * sub : (h + 1) * sub, :]
+
+    mine = ag.at[:, my_z, my_y, my_x]
     for d in reversed(near[1:]):
         back = (n_z - d) % n_z
         send(mine, mine, agz_send_sem, agz_recv_sem.at[back], tp_id(z_at(d) * 2 + my_c))
@@ -290,162 +322,176 @@
     def second_to(d, e):
         return kv_id(y_at(e), my_x) if x_first(d) else kv_id(my_y, x_at(e))
 
-    def spread_own(d):
-        block = ag.at[z_at(d), my_y, my_x]
-        if d:
-            await_bytes(block, agz_recv_sem.at[d])
+    def spread_own(h, d):
+        z = z_at(d)
+        block = ag.at[h, z, my_y, my_x]
+        if d and h == 0:
+            await_bytes(ag.at[:, z, my_y, my_x], agz_recv_sem.at[d])
         for e in side_far:
-            send(block, block, ag_send_sem.at[0], ag_recv_sem.at[0, d], first_to(d, e))
+            send(block, block, ag_send_sem.at[0], ag_recv_sem.at[0, h, d], first_to(d, e))
         for e in side_far:
-            send(block, block, ag_send_sem.at[1], ag_recv_sem.at[1, d], second_to(d, e))
-
-    def spread_on(d):
-        z = z_at(d)
-        await_bytes(ag.at[z, 0, pl.ds(0, n_side - 1)], ag_recv_sem.at[0, d])
+            send(block, block, ag_send_sem.at[1], ag_recv_sem.at[1, h, d], second_to(d, e))
+
+    def spread_on(h, d):
+        z = z_at(d)
+        await_bytes(ag.at[h, z, 0, pl.ds(0, n_side - 1)], ag_recv_sem.at[0, h, d])
         for e in side_far:
             for f in side_near:
-                block = ag.at[z, my_y, x_at(f)] if x_first(d) else ag.at[z, y_at(f), my_x]
-                send(block, block, ag_send_sem.at[1], ag_recv_sem.at[1, d], second_to(d, e))
-
-    batch = rows * n_side * n_side
-    sums = [jnp.zeros((batch, 4 * upad), F32), jnp.zeros((batch, 128), F32)]
-
-    def multiply(d):
-        z = z_at(d)
-        await_bytes(ag.at[z, pl.ds(0, n_side - 1)], ag_recv_sem.at[1, d])
-        lhs = ag[z].reshape(batch, fpd)
+                if x_first(d):
+                    block = ag.at[h, z, my_y, x_at(f)]
+                else:
+                    block = ag.at[h, z, y_at(f), my_x]
+                send(
+                    block, block, ag_send_sem.at[1], ag_recv_sem.at[1, h, d], second_to(d, e)
+                )
+
+    batch = sub * n_side * n_side
+    gate_up = [jnp.zeros((batch, 4 * upad), F32) for _ in range(parts)]
+    squares = [jnp.zeros((batch, 128), F32) for _ in range(parts)]
+    hidden = [None] * parts
+
+    def multiply(h, d):
+        z = z_at(d)
+        await_bytes(ag.at[h, z, pl.ds(0, n_side - 1)], ag_recv_sem.at[1, h, d])
+        lhs = ag[h, z].reshape(batch, fpd)
         wide = lhs.astype(F32)
         wide = wide * wide
         for q in range(fpd // 128):
-            sums[1] += wide[:, q * 128 : (q + 1) * 128]
-        sums[0] += lax.dot_general(
+            squares[h] += wide[:, q * 128 : (q + 1) * 128]
+        gate_up[h] += lax.dot_general(
             lhs, gu[z], (((1,), (1,)), ((), ())), preferred_element_type=F32
         )
 
-    steps = (
-        [(0, i) for i in range(3)]
-        + [(1, 0)]
-        + [(0, i) for i in range(3, n_z)]
-        + [(1, i) for i in range(1, n_z)]
-        + [(2, i) for i in range(n_z)]
-    )
-    for what, i in steps:
-        (spread_own, spread_on, multiply)[what](near[i])
-
-    ex_out[0] = sums[0][:, : 2 * upad].astype(BF16)
-    ex_out[1] = sums[0][:, 2 * upad :].astype(BF16)
-    exsq_out[...] = sums[1]
-    send(ex_out, ex_in, ex_send_sem.at[0], ex_recv_sem.at[0], tp_id(partner))
-    send(exsq_out, exsq_in, ex_send_sem.at[1], ex_recv_sem.at[1], tp_id(partner))
-    await_bytes(ex_in, ex_recv_sem.at[0])
-    await_bytes(exsq_in, ex_recv_sem.at[1])
-    row_scale = lax.rsqrt(
-        jnp.sum(sums[1] + exsq_in[...], axis=1, keepdims=True) / count + EPS
-    )
-    gate_far = pltpu.roll(ex_in[0].astype(F32), upad, 1)
-    up_far = pltpu.roll(ex_in[1].astype(F32), upad, 1)
-    gate_pre = (sums[0][:, : 2 * upad] + gate_far) * row_scale
-    up_pre = (sums[0][:, 2 * upad :] + up_far) * row_scale
-    hidden = (gate_pre / (1.0 + jnp.exp(-gate_pre)) * up_pre).astype(BF16)
-
-    def send_first(d):
+    def swap(h):
+        ex_out[h, 0] = gate_up[h][:, : 2 * upad].astype(BF16)
+        ex_out[h, 1] = gate_up[h][:, 2 * upad :].astype(BF16)
+        exsq_out[h] = squares[h]
+        send(ex_out.at[h], ex_in.at[h], ex_send_sem.at[0, h], ex_recv_sem.at[0, h], tp_id(partner))
+        send(
+            exsq_out.at[h], exsq_in.at[h], ex_send_sem.at[1, h], ex_recv_sem.at[1, h],
+            tp_id(partner),
+        )
+
+    def activate(h):
+        await_bytes(ex_in.at[h], ex_recv_sem.at[0, h])
+        await_bytes(exsq_in.at[h], ex_recv_sem.at[1, h])
+        row_scale = lax.rsqrt(
+            jnp.sum(squares[h] + exsq_in[h], axis=1, keepdims=True) / count + EPS
+        )
+        gate_far = pltpu.roll(ex_in[h, 0].astype(F32), upad, 1)
+        up_far = pltpu.roll(ex_in[h, 1].astype(F32), upad, 1)
+        gate_pre = (gate_up[h][:, : 2 * upad] + gate_far) * row_scale
+        up_pre = (gate_up[h][:, 2 * upad :] + up_far) * row_scale
+        hidden[h] = (gate_pre / (1.0 + jnp.exp(-gate_pre)) * up_pre).astype(BF16)
+
+    def project(h, d):
+        z = z_at(d)
+        down = jnp.dot(hidden[h], wd[z], preferred_element_type=F32)
+        pb[h, z] = down.astype(BF16).reshape(n_side, n_side, sub, fpd)
+
+    def send_first(h, d):
         z = z_at(d)
         for e in side_far:
             for f in side_near:
                 if x_first(d):
-                    block, slot, at = pb.at[z, y_at(e), x_at(f)], my_y, x_at(f)
+                    block, slot, at = pb.at[h, z, y_at(e), x_at(f)], my_y, x_at(f)
                 else:
-                    block, slot, at = pb.at[z, y_at(f), x_at(e)], my_x, y_at(f)
+                    block, slot, at = pb.at[h, z, y_at(f), x_at(e)], my_x, y_at(f)
                 send(
-                    block, r1.at[z, slot, at], r_send_sem.at[0], r_recv_sem.at[0, d],
+                    block, r1.at[h, z, slot, at], r_send_sem.at[0], r_recv_sem.at[0, h, d],
                     second_to(d, e),
                 )
 
-    def sum_first(d):
+    def sum_first(h, d):
         z = z_at(d)
         await_bytes(
-            r1.at[z, pl.ds(0, n_side - 1), pl.ds(0, n_side - 1)], r_recv_sem.at[0, d]
+            r1.at[h, z, pl.ds(0, n_side - 1), pl.ds(0, n_side - 1)], r_recv_sem.at[0, h, d]
         )
         for f in side_far:
             if x_first(d):
-                block, place, at = pb[z, my_y, x_at(f)], y_at, x_at(f)
+                block, place, at = pb[h, z, my_y, x_at(f)], y_at, x_at(f)
             else:
-                block, place, at = pb[z, y_at(f), my_x], x_at, y_at(f)
+                block, place, at = pb[h, z, y_at(f), my_x], x_at, y_at(f)
             block = block.astype(F32)
             for e in side_near:
-                block += r1[z, place(e), at].astype(F32)
-            mid[z, at] = block.astype(BF16)
-
-    def send_second(d):
+                block += r1[h, z, place(e), at].astype(F32)
+            mid[h, z, at] = block.astype(BF16)
+
+    def send_second(h, d):
         z = z_at(d)
         for e in side_far:
             at, slot = (x_at(e), my_x) if x_first(d) else (y_at(e), my_y)
             send(
-                mid.at[z, at], r2.at[z, slot], r_send_sem.at[1], r_recv_sem.at[1, d],
+                mid.at[h, z, at], r2.at[h, z, slot], r_send_sem.at[1], r_recv_sem.at[1, h, d],
                 first_to(d, e),
             )
         for e in side_far:
             if x_first(d):
-                block, slot = pb.at[z, y_at(e), my_x], r1.at[z, my_y, my_x]
+                block, slot = pb.at[h, z, y_at(e), my_x], r1.at[h, z, my_y, my_x]
             else:
-                block, slot = pb.at[z, my_y, x_at(e)], r1.at[z, my_x, my_y]
-            send(block, slot, r_send_sem.at[0], r_recv_sem.at[2, d], second_to(d, e))
-
-    def sum_second(d):
-        z = z_at(d)
-        await_bytes(r2.at[z, pl.ds(0, n_side - 1)], r_recv_sem.at[1, d])
-        await_bytes(r1.at[z, 0, pl.ds(0, n_side - 1)], r_recv_sem.at[2, d])
+                block, slot = pb.at[h, z, my_y, x_at(e)], r1.at[h, z, my_x, my_y]
+            send(block, slot, r_send_sem.at[0], r_recv_sem.at[2, h, d], second_to(d, e))
+
+    def sum_second(h, d):
+        z = z_at(d)
+        await_bytes(r2.at[h, z, pl.ds(0, n_side - 1)], r_recv_sem.at[1, h, d])
+        await_bytes(r1.at[h, z, 0, pl.ds(0, n_side - 1)], r_recv_sem.at[2, h, d])
         first, me_first, second = (x_at, my_x, y_at) if x_first(d) else (y_at, my_y, x_at)
-        block = pb[z, my_y, my_x].astype(F32)
+        block = pb[h, z, my_y, my_x].astype(F32)
         for e in side_near:
-            block += r1[z, second(e), me_first].astype(F32)
+            block += r1[h, z, second(e), me_first].astype(F32)
         for e in side_near:
-            block += r2[z, first(e)].astype(F32)
-        zout[z] = block.astype(BF16)
-
-    def send_third(d):
+            block += r2[h, z, first(e)].astype(F32)
+        zout[h, z] = block.astype(BF16)
+
+    def send_third(h, d):
         if d:
             send(
-                zout.at[z_at(d)], zin.at[my_z], rz_send_sem, rz_recv_sem,
+                zout.at[h, z_at(d)], zin.at[h, my_z], rz_send_sem, rz_recv_sem.at[h],
                 tp_id(z_at(d) * 2 + my_c),
             )
 
+    actions = {
+        "own": spread_own,
+        "on": spread_on,
+        "mm": multiply,
+        "swap": swap,
+        "act": activate,
+        "down": project,
+        "s1": send_first,
+        "a1": sum_first,
+        "s2": send_second,
+        "a2": sum_second,
+        "s3": send_third,
+    }
     far = list(reversed(near))
-    for i, d in enumerate(far):
-        z = z_at(d)
-        down = jnp.dot(hidden, wd[z], preferred_element_type=F32)
-        pb[z] = down.astype(BF16).reshape(n_side, n_side, rows, fpd)
-        if i:
-            send_first(far[i - 1])
-    send_first(far[-1])
-    lag = 4
-    for i in range(n_z + lag + 1):
-        if i < n_z:
-            sum_first(far[i])
-        if 0 <= i - 1 < n_z:
-            send_second(far[i - 1])
-        if 0 <= i - lag < n_z:
-            sum_second(far[i - lag])
-        if 0 <= i - lag - 1 < n_z:
-            send_third(far[i - lag - 1])
-    out = residual.astype(F32) + zout[my_z].astype(F32)
-    await_bytes(zin.at[pl.ds(0, n_z - 1)], rz_recv_sem)
-    for d in near[1:]:
-        out += zin[z_at(d)].astype(F32)
-    result_out[...] = out.astype(BF16)
+    for what, h, *which in schedule(n_z, parts):
+        if which:
+            order = far if what in ("down", "s1", "a1", "s2", "a2", "s3") else near
+            actions[what](h, order[which[0]])
+        else:
+            actions[what](h)
+
+    for h in range(parts):
+        out = residual[h * sub : (h + 1) * sub, :].astype(F32) + zout[h, my_z].astype(F32)
+        await_bytes(zin.at[h, pl.ds(0, n_z - 1)], rz_recv_sem.at[h])
+        for d in near[1:]:
+            out += zin[h, z_at(d)].astype(F32)
+        result_out[h * sub : (h + 1) * sub, :] = out.astype(BF16)
 
     await_bytes(tok_all.at[pl.ds(0, n_tp - 1)], tok_send_sem)
     for j in range(3):
         await_bytes(far_w.at[j], far_send_sem.at[j])
     await_bytes(recv1.at[pl.ds(0, n_tp - 1)], p1_send_sem)
-    await_bytes(zin.at[pl.ds(0, n_z - 1)], agz_send_sem)
-    await_bytes(ag.at[:, 0, pl.ds(0, n_side - 1)], ag_send_sem.at[0])
-    await_bytes(ag.at[:, pl.ds(0, n_side - 1)], ag_send_sem.at[1])
-    await_bytes(ex_in, ex_send_sem.at[0])
-    await_bytes(exsq_in, ex_send_sem.at[1])
-    await_bytes(ag.at[:, pl.ds(0, n_side - 1)], r_send_sem.at[0])
-    await_bytes(ag.at[:, 0, pl.ds(0, n_side - 1)], r_send_sem.at[1])
-    await_bytes(zin.at[pl.ds(0, n_z - 1)], rz_send_sem)
+    await_bytes(zin.at[:, pl.ds(0, n_z - 1)], agz_send_sem)
+    await_bytes(ag.at[:, :, 0, pl.ds(0, n_side - 1)], ag_send_sem.at[0])
+    await_bytes(ag.at[:, :, pl.ds(0, n_side - 1)], ag_send_sem.at[1])
+    for h in range(parts):
+        await_bytes(ex_in.at[h], ex_send_sem.at[0, h])
+        await_bytes(exsq_in.at[h], ex_send_sem.at[1, h])
+    await_bytes(ag.at[:, :, pl.ds(0, n_side - 1)], r_send_sem.at[0])
+    await_bytes(ag.at[:, :, 0, pl.ds(0, n_side - 1)], r_send_sem.at[1])
+    await_bytes(zin.at[:, pl.ds(0, n_z - 1)], rz_send_sem)
 
 
 def write_kernel(result_ref, ns_ref, result_out, ns_out, sem):
@@ -486,15 +532,16 @@
         head = w_query.shape[1]
         units = w_gate.shape[1]
         upad = 64
-        batch = rows * n_kv
+        parts = 1
+        sub = rows // parts
+        batch = sub * n_kv
         hbm = pl.BlockSpec(memory_space=pl.ANY)
         out_hbm = pl.BlockSpec(memory_space=pltpu.VMEM)
-        smem = pl.BlockSpec(memory_space=pltpu.SMEM)
         dma = pltpu.SemaphoreType.DMA
         vmem = pltpu.VMEM
 
         def kernel(*refs):
-            layer_kernel(n_side, n_z, *refs)
+            layer_kernel(n_side, n_z, parts, *refs)
 
         operands = (
             tokens,
@@ -504,7 +551,7 @@
             w_value,
             w_outgate,
             w_rates.reshape(2, feats),
-            head_rate,
+            head_rate.reshape(1, 1),
             head_gain.reshape(1, head),
             w_out,
             state.reshape(rows, head, head),
@@ -514,7 +561,7 @@
             w_down.T,
         )
         operands = [
-            a if a is head_rate else pltpu.with_memory_space_constraint(a, pltpu.HBM)
+            pltpu.with_memory_space_constraint(a, pltpu.HBM) if a.size > 1 else a
             for a in operands
         ]
         result, new_state = pl.pallas_call(
@@ -524,7 +571,7 @@
                 jax.ShapeDtypeStruct((rows, fpd), BF16),
                 jax.ShapeDtypeStruct((rows, head, head), F32),
             ),
-            in_specs=[hbm] * 7 + [smem] + [hbm] * 7,
+            in_specs=[hbm] * 15,
             out_specs=(out_hbm, out_hbm),
             scratch_shapes=[
                 vmem((rows, fpd), BF16),
@@ -536,6 +583,7 @@
                 vmem((1, feats), F32),
                 vmem((1, feats), F32),
                 vmem((1, head), F32),
+                vmem((1, 1), F32),
                 vmem((2, feats), BF16),
                 vmem((3, units, feats), BF16),
                 vmem((3, units, feats), BF16),
@@ -543,34 +591,34 @@
                 vmem((n_z, 2 * upad, fpd), BF16),
                 vmem((n_tp, rows, fpd), BF16),
                 vmem((n_tp, rows, fpd), BF16),
-                vmem((n_z, n_side, n_side, rows, fpd), BF16),
-                vmem((2, batch, 2 * upad), BF16),
-                vmem((2, batch, 2 * upad), BF16),
-                vmem((batch, 128), F32),
-                vmem((batch, 128), F32),
-                vmem((n_z, n_side, n_side, rows, fpd), BF16),
-                vmem((n_z, n_side, n_side, rows, fpd), BF16),
-                vmem((n_z, n_side, rows, fpd), BF16),
-                vmem((n_z, n_side, rows, fpd), BF16),
-                vmem((n_z, rows, fpd), BF16),
-                vmem((n_z, rows, fpd), BF16),
-                dma((14,)),
+                vmem((parts, n_z, n_side, n_side, sub, fpd), BF16),
+                vmem((parts, 2, batch, 2 * upad), BF16),
+                vmem((parts, 2, batch, 2 * upad), BF16),
+                vmem((parts, batch, 128), F32),
+                vmem((parts, batch, 128), F32),
+                vmem((parts, n_z, n_side, n_side, sub, fpd), BF16),
+                vmem((parts, n_z, n_side, n_side, sub, fpd), BF16),
+                vmem((parts, n_z, n_side, sub, fpd), BF16),
+                vmem((parts, n_z, n_side, sub, fpd), BF16),
+                vmem((parts, n_z, sub, fpd), BF16),
+                vmem((parts, n_z, sub, fpd), BF16),
+                dma((15,)),
                 dma((3,)),
                 dma((3,)),
                 dma,
-                dma((3,)),
+                dma((n_z // 2,)),
                 dma,
                 dma,
                 dma,
                 dma((n_z,)),
                 dma((2,)),
-                dma((2, n_z)),
+                dma((2, parts, n_z)),
+                dma((2, parts)),
+                dma((2, parts)),
                 dma((2,)),
-                dma((2,)),
-                dma((2,)),
-                dma((3, n_z)),
+                dma((3, parts, n_z)),
                 dma,
-                dma,
+                dma((parts,)),
             ],
             compiler_params=pltpu.CompilerParams(
                 collective_id=0,

time: 56 us -> 54.8 us (0.979)
  Pallas kernels: 54.5 us -> 53.3 us
    pallas_call x1, Pallas kernels: 53.5 us -> 52.3 us  [body(): pl.pallas_call(kernel, name='layer', out_shape=(jax.ShapeDtypeStruct((row...]
where the time goes in v3:
time: 54.8 us; the launch traced here: 54.6 us
  Pallas kernels  53.3 us (97%)
  between operations  1.29 us (2%)
    pallas_call x1, Pallas kernels, body(): pl.pallas_call(kernel, name='layer', out_shape=(jax.ShapeDtypeStruct((row...  52.3 us

profile of v3, /device:TPU:1, one launch (start us, length us, event | category | flops | bytes accessed | tf_op | source)
XLA Modules:
  0.0 54.6 jit_solution(15113677029818646095)
XLA Ops:
  1.3 52.3 %layer.1 = (bf16[16,256]{1,0:T(8,128)(2,1)S(1)}, f32[16,128,128]{2,1,0:T(8,128)S(1)}) custom-call(bf16[16,256]{1,0:T(8,128)(2,1)} %refs_0_.1, f32[1,4096]{1,0:T(1,128)} %bitcast.17, bf16[4096,128]{1,0:T(8,128)(2,1)} %refs_2_.1, bf16[4096,128]{1,0:T(8,128)(2,1)} %refs_3_.1, bf16[4096,128]{1,0:T(8,128)(2,1)} %refs_4_.1, bf16[4096,128]{1,0:T(8,128)(2,1)} %refs_5_.1, ...), custom_call_target="tpu_custom_call" | custom-call | tf_op jit(solution)/shard_map/layer/pallas_call | solution.py:567
  53.6 1.0 %write.1 = (bf16[16,256]{1,0:T(8,128)(2,1)}, f32[16,128,128]{2,1,0:T(8,128)}) custom-call(bf16[16,256]{1,0:T(8,128)(2,1)S(1)} %get-tuple-element.6.result_ref, f32[16,128,128]{2,1,0:T(8,128)S(1)} %get-tuple-element.7.ns_ref), custom_call_target="tpu_custom_call" | custom-call | tf_op jit(solution)/shard_map/write/pallas_call | solution.py:629
